TPU v7x, 32 devices: a whole 2x2x4 slice. The times are simulated.
32 devices in a mesh: sp: 8 (over z, x), tp: 4 (over y, core).
Axes of the slice: x: 2, y: 2, z: 4, core: 2. Of those that a mesh axis runs over, the one named last changes fastest.
Arguments:
- residual: bfloat16 [4096, 2048], P(('sp', 'tp')), may hold values from -6 to 6
- conv_value: bfloat16 [4096, 1024], P('sp', 'tp'), may hold values from -6 to 6
- conv_gate: bfloat16 [4096, 1024], P('sp', 'tp'), may hold values from -9 to 9
- segments: int32 [4096], P('sp'), may hold values from 0 to 3, never falling along the last dimension, each value on 1 to 2048 neighbouring positions
- conv_weight: float32 [31, 1024], P(None, 'tp'), may hold values from -1 to 1
- norm_gain: float32 [1024], P('tp'), may hold values from 0.1 to 1.9
- norm_shift: float32 [1024], P('tp'), may hold values from -3 to 3
- out_weight: bfloat16 [1024, 2048], replicated, may hold values from -0.1875 to 0.1875
- ffn_gain: float32 [2048], replicated, may hold values from 0.1 to 1.9
- routes: int32 [4096, 2], P('sp'), may hold values from 0 to 7, all different within a row; in each aligned block of 128 rows (0 to 127, 128 to 255, ...) at most 64 rows name the same one
- route_weights: float32 [4096, 2], P('sp'), may hold values from 0.2 to 1
- w_gate: bfloat16 [8, 2048, 1024], P('sp', None, 'tp'), may hold values from -0.125 to 0.125
- w_up: bfloat16 [8, 2048, 1024], P('sp', None, 'tp'), may hold values from -0.125 to 0.125
- w_down: bfloat16 [8, 1024, 2048], P('sp', 'tp'), may hold values from -0.1875 to 0.1875
Outputs:
- layer_out: bfloat16 [4096, 2048], P(('sp', 'tp'))
Inputs may be any that keep to these rules, and one draw needn't show every extreme that they name: `routes`: within the rows of one device (aligned blocks of 512 / 4 rows), no expert is named more than 64 times; the two experts of a row differ. `segments`: document numbers never fall along the sequence.
All inputs are finite; a program needn't handle non-finite values.
Results may differ from a plain program's by a relative error of at most 0.007.
Values may be sent and summed in bfloat16 or wider, within the bound.
A program may use at most 128 MiB of HBM per device.

v0:
```python
import jax
import jax.numpy as jnp
from jax import lax
from jax.sharding import PartitionSpec as P

DC = 1024
CONV_GROUPS = 8


def passed_along(value, axis, steps):
    count = lax.axis_size(axis)
    initial, last = (max(0, -steps), min(count, count - steps))
    return lax.ppermute(value, axis, [(source, source + steps) for source in range(initial, last)])


def slot_numbers(block_routes, capacity, experts_n):
    route_pairs = block_routes.reshape(block_routes.shape[:-2] + (-1,))
    onehot = (route_pairs[..., None] == jnp.arange(experts_n, dtype=jnp.int32)).astype(jnp.int32)
    slot_rank = jnp.sum((jnp.cumsum(onehot, axis=-2) - onehot) * onehot, axis=-1)
    return (route_pairs * capacity + slot_rank).reshape(block_routes.shape)


def dispatch_matrix(slot_ids, slot_total):
    numbers = jnp.arange(slot_total, dtype=jnp.int32)[:, None, None]
    matches = jnp.any(numbers == slot_ids[..., None, :, :], axis=-1)
    return matches.astype(jnp.bfloat16)


def shards(
    residual,
    conv_value,
    conv_gate,
    segments,
    conv_weight,
    norm_gain,
    norm_shift,
    out_weight,
    ffn_gain,
    routes,
    route_weights,
    w_gate,
    w_up,
    w_down,
):
    tok_dev, local_channels = conv_value.shape
    reach = conv_weight.shape[0] - 1
    whole_gate, whole_up = (
        lax.all_gather(w_gate[0], "tp", axis=1, tiled=True),
        lax.all_gather(w_up[0], "tp", axis=1, tiled=True),
    )
    whole_down = lax.all_gather(w_down[0], "tp", axis=0, tiled=True)
    gated = (conv_value.astype(jnp.float32) * jax.nn.sigmoid(conv_gate.astype(jnp.float32))).astype(
        jnp.bfloat16
    )
    rim_prev, seg_prev = passed_along(
        (gated[tok_dev - reach :], segments[tok_dev - reach :]), "sp", 1
    )
    extended = jnp.concatenate([rim_prev, gated], 0).astype(jnp.float32)
    seg_ext = jnp.concatenate([seg_prev, segments], 0)
    convolved = jnp.zeros((tok_dev, local_channels), jnp.float32)
    for offset in range(reach + 1):
        same_doc = (seg_ext[offset : offset + tok_dev] == segments)[:, None]
        convolved = convolved + jnp.where(
            same_doc, extended[offset : offset + tok_dev] * conv_weight[offset], 0.0
        )
    group_size = DC // CONV_GROUPS
    grouped = convolved.reshape(tok_dev, local_channels // group_size, group_size)
    group_mean = jnp.mean(grouped, axis=-1, keepdims=True)
    group_var = jnp.mean(jnp.square(grouped - group_mean), axis=-1, keepdims=True)
    scaled = ((grouped - group_mean) * lax.rsqrt(group_var + 1e-05)).reshape(
        tok_dev, local_channels
    ) * norm_gain + norm_shift
    conv_out = jax.nn.silu(scaled).astype(jnp.bfloat16)
    columns = lax.axis_size("tp")
    column = lax.axis_index("tp")
    rows_own = tok_dev // columns
    weight_rows = lax.dynamic_slice_in_dim(out_weight, column * local_channels, local_channels, 0)
    mixed = lax.psum_scatter(
        jnp.dot(conv_out, weight_rows, preferred_element_type=jnp.float32),
        "tp",
        scatter_dimension=0,
        tiled=True,
    )
    stream = residual.astype(jnp.float32) + lax.optimization_barrier(
        mixed.astype(jnp.bfloat16)
    ).astype(jnp.float32)
    normed = (
        stream * lax.rsqrt(jnp.mean(stream * stream, axis=-1, keepdims=True) + 1e-06) * ffn_gain
    ).astype(jnp.bfloat16)
    experts_n = lax.axis_size("sp")
    top_count = routes.shape[1]
    model_width = normed.shape[1]
    capacity = max(2, 2 * tok_dev * top_count // (columns * experts_n))
    slot_total = experts_n * capacity
    own_routes = lax.dynamic_slice_in_dim(routes, column * rows_own, rows_own, 0)
    own_weights = lax.dynamic_slice_in_dim(route_weights, column * rows_own, rows_own, 0)
    own_slots = slot_numbers(own_routes, capacity, experts_n)
    routing_table = dispatch_matrix(own_slots, slot_total)
    outgoing = jnp.dot(routing_table, normed, preferred_element_type=jnp.float32).astype(
        jnp.bfloat16
    )
    outgoing = outgoing.reshape(experts_n, capacity, model_width)
    arrived = lax.all_to_all(outgoing, "sp", split_axis=0, concat_axis=1, tiled=True).reshape(
        slot_total, model_width
    )
    gate_act = jnp.dot(arrived, whole_gate, preferred_element_type=jnp.float32)
    up_act = jnp.dot(arrived, whole_up, preferred_element_type=jnp.float32)
    hidden = (jax.nn.silu(gate_act) * up_act).astype(jnp.bfloat16)
    summed = jnp.dot(hidden, whole_down, preferred_element_type=jnp.float32)
    expert_out = summed.astype(jnp.bfloat16).reshape(experts_n, capacity, model_width)
    returned = lax.all_to_all(expert_out, "sp", split_axis=0, concat_axis=0, tiled=True).reshape(
        slot_total, model_width
    )
    combined = stream
    for member in range(top_count):
        chosen = jnp.take(returned, own_slots[:, member], axis=0).astype(jnp.float32)
        combined = combined + own_weights[:, member : member + 1] * chosen
    return combined.astype(jnp.bfloat16)


def solution(mesh):
    return jax.shard_map(
        shards,
        mesh=mesh,
        in_specs=(
            P(("sp", "tp"), None),
            P("sp", "tp"),
            P("sp", "tp"),
            P("sp"),
            P(None, "tp"),
            P("tp"),
            P("tp"),
            P(),
            P(),
            P("sp", None),
            P("sp", None),
            P("sp", None, "tp"),
            P("sp", None, "tp"),
            P("sp", "tp", None),
        ),
        out_specs=P(("sp", "tp"), None),
        check_vma=False,
    )
```

profile of v0, /device:TPU:0, one launch (start us, length us, event | category | flops | bytes accessed | tf_op | source)
XLA Modules:
  0.0 263.9 jit_solution(16011926092684907815)
XLA Ops:
  7.3 4.9 %collective-permute-start = (s32[30]{0:T(128)S(1)}, s32[30]{0:T(128)S(1)}, u32[]{:S(2)}, u32[]{:S(2)}) collective-permute-start(s32[30]{0:T(128)S(1)} %slice.300), channel_id=1, source_target_pairs={{0,4},{4,8},{8,12},{12,16},{16,20},{20,24},{24,28},{1,5},{5,9},{9,... | collective-permute-start | bytes 368 | tf_op jit(solution)/shard_map/ppermute | solution.py:13
  12.2 1.2 multiply_convert_fusion.4
  13.4 3.5 %collective-permute-start.1 = (bf16[30,256]{1,0:T(8,128)(2,1)S(1)}, bf16[30,256]{1,0:T(8,128)(2,1)S(1)}, u32[]{:S(2)}, u32[]{:S(2)}) collective-permute-start(bf16[30,256]{1,0:T(8,128)(2,1)S(1)} %slice.404), channel_id=1, source_target_pairs={{0,4},{4,8},{8,12},{12,16},{16,20},{20,24},{24,28},{1,5},{5,9},{9,... | collective-permute-start | bytes 46088 | tf_op jit(solution)/shard_map/ppermute | solution.py:13
  16.8 1.0 fusion.89
  17.9 1.0 fusion.90
  19.6 0.8 slice_compare_fusion.29
  21.2 4.0 %fusion.17 = f32[512,256]{1,0:T(8,128)S(1)} fusion(f32[542,256]{1,0:T(8,128)S(1)} %maximum_convert_fusion, f32[256]{0:T(256)S(1)} %bitcast.119, f32[256]{0:T(256)S(1)} %bitcast.120, f32[256]{0:T(256)S(1)} %bitcast.91, f32[256]{0:T(256)S(1)} %bitcast.92, f32[256]{0:T(256)S(1)} %bitcast.93, f32[256]{0:T(256)S(1)} %bitcast.94, f32[256]{0:T(256)S(1)} %bitcast.95, ...), kind=kLoop, calls=%fused_computation.22 | loop fusion | flops 11927552 | bytes 16824320 | tf_op jit(solution)/shard_map/add | solution.py:63
  26.2 1.6 multiply_reduce_fusion.1
  29.1 4.0 %fusion.11 = f32[512,2048]{1,0:T(8,128)} fusion(bf16[1024,2048]{1,0:T(8,128)(2,1)} %param.23, s32[]{:T(128)S(6)} %select_n.136, f32[64,8,2,128]{3,2,1,0:T(2,128)S(1)} %bitcast.85, f32[512,256]{1,0:T(8,128)S(1)} %fusion.17, f32[64,8,2,128]{3,2,1,0:T(2,128)S(1)} %bitcast.86, f32[256]{0:T(256)S(1)} %copy-done.3, f32[256]{0:T(256)S(1)} %copy-done.4), kind=kOutput, calls=%fused_computation.15 | convolution fusion | flops 538050560 | bytes 6817796 | tf_op jit(solution)/shard_map/dot_general | solution.py:79
  36.9 41.2 %reduce-scatter.2.cloned.1.call-done = f32[128,2048]{1,0:T(8,128)} async-done(((f32[512,2048]{1,0:T(8,128)}), f32[128,2048]{1,0:T(8,128)}) %reduce-scatter.2.cloned.1.call-update) | async-done | bytes 1048592 | tf_op jit(solution)/shard_map/reduce_scatter | solution.py:78
  78.1 1.3 convert_element_type.59
  79.7 2.2 convolution_convert_fusion
  81.8 5.5 %all-to-all-start = ((bf16[8,64,2048]{2,1,0:T(8,128)(2,1)}), bf16[8,64,2048]{2,1,0:T(8,128)(2,1)S(1)}, u32[]{:S(2)}, u32[]{:S(2)}) async-start(bf16[8,64,2048]{2,1,0:T(8,128)(2,1)} %bitcast.34), calls=%async_computation.1 | async-start | bytes 4194304 | tf_op jit(solution)/shard_map/all_to_all | solution.py:103
  87.3 27.3 %all-gather.7.cloned.1.call-done = bf16[1,2048,1024]{2,1,0:T(8,128)(2,1)} async-done(((bf16[1,2048,256]{2,1,0:T(8,128)(2,1)}), bf16[1,2048,1024]{2,1,0:T(8,128)(2,1)}) %all-gather.7.cloned.1.call-update) | async-done | bytes 4194320 | tf_op jit(solution)/shard_map/all_gather | solution.py:48
  114.7 20.7 %all-to-all-done = bf16[8,64,2048]{2,1,0:T(8,128)(2,1)S(1)} async-done(((bf16[8,64,2048]{2,1,0:T(8,128)(2,1)}), bf16[8,64,2048]{2,1,0:T(8,128)(2,1)S(1)}, u32[]{:S(2)}, u32[]{:S(2)}) %all-to-all-start) | async-done | bytes 2097184 | tf_op jit(solution)/shard_map/all_to_all | solution.py:103
  135.4 6.0 %fusion.4 = f32[512,1024]{1,0:T(8,128)} fusion(bf16[512,2048]{1,0:T(8,128)(2,1)S(1)} %bitcast.88, bf16[1,2048,1024]{2,1,0:T(8,128)(2,1)} %all-gather.7.cloned.1.call-done), kind=kOutput, calls=%fused_computation.6 | convolution fusion | flops 2147483648 | bytes 8388608 | tf_op jit(solution)/shard_map/dot_general | solution.py:106
  141.4 9.4 %all-gather.11.cloned.1.call-done = bf16[1,1024,2048]{2,1,0:T(8,128)(2,1)} async-done(((bf16[1,256,2048]{2,1,0:T(8,128)(2,1)}), bf16[1,1024,2048]{2,1,0:T(8,128)(2,1)}) %all-gather.11.cloned.1.call-update) | async-done | bytes 4194320 | tf_op jit(solution)/shard_map/all_gather | solution.py:51
  150.8 36.4 %all-gather.9.cloned.1.call-done = bf16[1,2048,1024]{2,1,0:T(8,128)(2,1)} async-done(((bf16[1,2048,256]{2,1,0:T(8,128)(2,1)}), bf16[1,2048,1024]{2,1,0:T(8,128)(2,1)}) %all-gather.9.cloned.1.call-update) | async-done | bytes 4194320 | tf_op jit(solution)/shard_map/all_gather | solution.py:49
  187.2 10.0 %fusion.6 = bf16[512,2048]{1,0:T(8,128)(2,1)} fusion(bf16[1,1024,2048]{2,1,0:T(8,128)(2,1)} %all-gather.11.cloned.1.call-done, f32[512,1024]{1,0:T(8,128)} %fusion.4, bf16[512,2048]{1,0:T(8,128)(2,1)S(1)} %bitcast.89, bf16[1,2048,1024]{2,1,0:T(8,128)(2,1)} %all-gather.9.cloned.1.call-done), kind=kOutput, calls=%fused_computation.8 | convolution fusion | flops 4299161600 | bytes 14680064 | tf_op jit(solution)/shard_map/dot_general | solution.py:109
  197.2 5.5 %all-to-all-start.1 = ((bf16[8,64,2048]{2,1,0:T(8,128)(2,1)}), bf16[8,64,2048]{2,1,0:T(8,128)(2,1)S(1)}, u32[]{:S(2)}, u32[]{:S(2)}) async-start(bf16[8,64,2048]{2,1,0:T(8,128)(2,1)} %bitcast.87), calls=%async_computation.2 | async-start | bytes 4194304 | tf_op jit(solution)/shard_map/all_to_all | solution.py:111
  203.7 47.7 %all-to-all-done.1 = bf16[8,64,2048]{2,1,0:T(8,128)(2,1)S(1)} async-done(((bf16[8,64,2048]{2,1,0:T(8,128)(2,1)}), bf16[8,64,2048]{2,1,0:T(8,128)(2,1)S(1)}, u32[]{:S(2)}, u32[]{:S(2)}) %all-to-all-start.1) | async-done | bytes 2097184 | tf_op jit(solution)/shard_map/all_to_all | solution.py:111
  251.4 1.7 gather_fusion
  253.1 1.7 gather_fusion.1
  254.8 2.5 add_convert_fusion
  (54 shorter events, 9.3 us)
Async XLA Ops:
  6.5 28.7 %copy-start = (s32[512,2]{0,1:T(2,128)S(1)}, s32[512,2]{0,1:T(2,128)}, u32[]{:S(2)}) copy-start(s32[512,2]{0,1:T(2,128)} %param.25) | copy-start | bytes 12292
  6.5 71.6 %reduce-scatter.2.cloned.1.call-start = ((), (), s32[]{:S(2)}) async-start(), calls=%async_computation.3 | async-start | bytes 5242880 | tf_op jit(solution)/shard_map/reduce_scatter | solution.py:78
  7.3 11.5 %collective-permute-start = (s32[30]{0:T(128)S(1)}, s32[30]{0:T(128)S(1)}, u32[]{:S(2)}, u32[]{:S(2)}) collective-permute-start(s32[30]{0:T(128)S(1)} %slice.300), channel_id=1, source_target_pairs={{0,4},{4,8},{8,12},{12,16},{16,20},{20,24},{24,28},{1,5},{5,9},{9,... | collective-permute-start | bytes 368 | tf_op jit(solution)/shard_map/ppermute | solution.py:13
  13.4 7.8 %collective-permute-start.1 = (bf16[30,256]{1,0:T(8,128)(2,1)S(1)}, bf16[30,256]{1,0:T(8,128)(2,1)S(1)}, u32[]{:S(2)}, u32[]{:S(2)}) collective-permute-start(bf16[30,256]{1,0:T(8,128)(2,1)S(1)} %slice.404), channel_id=1, source_target_pairs={{0,4},{4,8},{8,12},{12,16},{16,20},{20,24},{24,28},{1,5},{5,9},{9,... | collective-permute-start | bytes 46088 | tf_op jit(solution)/shard_map/ppermute | solution.py:13
  25.6 3.5 %copy-start.3 = (f32[256]{0:T(256)S(1)}, f32[256]{0:T(256)}, u32[]{:S(2)}) copy-start(f32[256]{0:T(256)} %param.22) | copy-start | bytes 3076
  25.6 3.5 %copy-start.4 = (f32[256]{0:T(256)S(1)}, f32[256]{0:T(256)}, u32[]{:S(2)}) copy-start(f32[256]{0:T(256)} %param.21) | copy-start | bytes 3076
  33.1 81.6 %all-gather.7.cloned.1.call-start = ((), (), s32[]{:S(2)}) async-start(), calls=%async_computation.4 | async-start | bytes 5242880 | tf_op jit(solution)/shard_map/all_gather | solution.py:48
  33.9 45.5 %copy-start.1 = (bf16[128,2048]{1,0:T(8,128)(2,1)S(1)}, bf16[128,2048]{1,0:T(8,128)(2,1)}, u32[]{:S(2)}) copy-start(bf16[128,2048]{1,0:T(8,128)(2,1)} %param.16) | copy-start | bytes 1572868
  33.9 116.9 %all-gather.11.cloned.1.call-start = ((), (), s32[]{:S(2)}) async-start(), calls=%async_computation.6 | async-start | bytes 5242880 | tf_op jit(solution)/shard_map/all_gather | solution.py:51
  34.6 45.0 %copy-start.2 = (f32[2048]{0:T(1024)S(1)}, f32[2048]{0:T(1024)}, u32[]{:S(2)}) copy-start(f32[2048]{0:T(1024)} %param.24) | copy-start | bytes 24580
  34.6 152.6 %all-gather.9.cloned.1.call-start = ((), (), s32[]{:S(2)}) async-start(), calls=%async_computation.5 | async-start | bytes 5242880 | tf_op jit(solution)/shard_map/all_gather | solution.py:49
  81.8 53.6 %all-to-all-start = ((bf16[8,64,2048]{2,1,0:T(8,128)(2,1)}), bf16[8,64,2048]{2,1,0:T(8,128)(2,1)S(1)}, u32[]{:S(2)}, u32[]{:S(2)}) async-start(bf16[8,64,2048]{2,1,0:T(8,128)(2,1)} %bitcast.34), calls=%async_computation.1 | async-start | bytes 4194304 | tf_op jit(solution)/shard_map/all_to_all | solution.py:103
  197.2 54.2 %all-to-all-start.1 = ((bf16[8,64,2048]{2,1,0:T(8,128)(2,1)}), bf16[8,64,2048]{2,1,0:T(8,128)(2,1)S(1)}, u32[]{:S(2)}, u32[]{:S(2)}) async-start(bf16[8,64,2048]{2,1,0:T(8,128)(2,1)} %bitcast.87), calls=%async_computation.2 | async-start | bytes 4194304 | tf_op jit(solution)/shard_map/all_to_all | solution.py:111
Sparse Core Ops, SparseCore 0:
  33.2 44.8 reduce-scatter.1
  79.7 34.9 all-gather.6
  116.3 34.4 all-gather.10
  152.2 34.9 all-gather.8
where the time goes:
time: 265 us; the launch traced here: 264 us
  waiting for transfers between devices  185 us (70%)
  matrix products  22.1 us (8%)
  starting transfers between devices  19.5 us (7%)
  other arithmetic  14.7 us (6%)
  between operations  13.4 us (5%)
  local copies, waits for them, and re-layouts  9.39 us (4%)
    all_to_all x1, waiting for transfers between devices, shards(): lax.all_to_all(expert_out, 'sp', split_axis=0, concat_axis=0, tiled=True)  47.7 us
    reduce_scatter x1, waiting for transfers between devices, shards(): lax.psum_scatter(jnp.dot(conv_out, weight_rows, preferred_element_type=jn...  41.2 us
    all_gather x1, waiting for transfers between devices, shards(): lax.all_gather(w_up[0], 'tp', axis=1, tiled=True)  36.4 us
    all_gather x1, waiting for transfers between devices, shards(): lax.all_gather(w_gate[0], 'tp', axis=1, tiled=True)  27.3 us
    all_to_all x1, waiting for transfers between devices, shards(): lax.all_to_all(outgoing, 'sp', split_axis=0, concat_axis=1, tiled=True)  20.7 us
    dot_general x1, matrix products, shards(): summed = jnp.dot(hidden, whole_down, preferred_element_type=jnp.float32)  10 us
    all_gather x1, waiting for transfers between devices, shards(): whole_down = lax.all_gather(w_down[0], 'tp', axis=0, tiled=True)  9.38 us
    ppermute x2, starting transfers between devices, passed_along(): lax.ppermute(value, axis, [(source, source + steps) for source in range(i...  8.32 us
  transfers between devices with their start and end apart: 8, of which 6 were waited for; matrix products, arithmetic and copies ran while one was open for 7% of the time, Pallas kernels for 0%

commit v1 on v0

--- a/solution.py
+++ b/solution.py
@@ -5,6 +5,29 @@
 
 DC = 1024
 CONV_GROUPS = 8
+
+
+def cut_along(value, dim, size):
+    shape = value.shape
+    blocks = value.reshape(*shape[:dim], size, shape[dim] // size, *shape[dim + 1 :])
+    return jnp.moveaxis(blocks, dim, 0)
+
+
+def laid_out(tiles, dim):
+    shape = list(tiles.shape[1:])
+    shape[dim] *= tiles.shape[0]
+    return jnp.moveaxis(tiles, 0, dim).reshape(shape)
+
+
+def exchange_in_pairs(x, axis, split_dim, concat_dim):
+    size, index = (lax.axis_size(axis), lax.axis_index(axis))
+    parts = cut_along(x, split_dim, size)
+    finished = [parts[index]]
+    for lap in range(1, size):
+        sent = parts[index ^ lap]
+        finished.append(lax.ppermute(sent, axis, [(i, i ^ lap) for i in range(size)]))
+    parts = jnp.stack(finished)[index ^ jnp.arange(size)]
+    return laid_out(parts, concat_dim)
 
 
 def passed_along(value, axis, steps):
@@ -108,9 +131,7 @@
     hidden = (jax.nn.silu(gate_act) * up_act).astype(jnp.bfloat16)
     summed = jnp.dot(hidden, whole_down, preferred_element_type=jnp.float32)
     expert_out = summed.astype(jnp.bfloat16).reshape(experts_n, capacity, model_width)
-    returned = lax.all_to_all(expert_out, "sp", split_axis=0, concat_axis=0, tiled=True).reshape(
-        slot_total, model_width
-    )
+    returned = exchange_in_pairs(expert_out, "sp", 0, 0).reshape(slot_total, model_width)
     combined = stream
     for member in range(top_count):
         chosen = jnp.take(returned, own_slots[:, member], axis=0).astype(jnp.float32)

time: 265 us -> 265 us (level)
  the two profiles are of different devices: /device:TPU:0 before, /device:TPU:16 now
where the time goes in v1:
time: 265 us; the launch traced here: 264 us
  waiting for transfers between devices  179 us (68%)
  matrix products  22 us (8%)
  starting transfers between devices  21.4 us (8%)
  other arithmetic  14.7 us (6%)
  between operations  13.5 us (5%)
  local copies, waits for them, and re-layouts  13.4 us (5%)
    ppermute x7, waiting for transfers between devices, exchange_in_pairs(): lax.ppermute(sent, axis, [(i, i ^ lap) for i in range(size)])  43.8 us
    reduce_scatter x1, waiting for transfers between devices, shards(): lax.psum_scatter(jnp.dot(conv_out, weight_rows, preferred_element_type=jn...  41 us
    all_gather x1, waiting for transfers between devices, shards(): lax.all_gather(w_up[0], 'tp', axis=1, tiled=True)  36.4 us
    all_gather x1, waiting for transfers between devices, shards(): lax.all_gather(w_gate[0], 'tp', axis=1, tiled=True)  26.6 us
    all_to_all x1, waiting for transfers between devices, shards(): lax.all_to_all(outgoing, 'sp', split_axis=0, concat_axis=1, tiled=True)  17.9 us
    all_gather x1, waiting for transfers between devices, shards(): whole_down = lax.all_gather(w_down[0], 'tp', axis=0, tiled=True)  11.5 us
    dot_general x1, matrix products, shards(): summed = jnp.dot(hidden, whole_down, preferred_element_type=jnp.float32)  9.23 us
    ppermute x7, starting transfers between devices, exchange_in_pairs(): lax.ppermute(sent, axis, [(i, i ^ lap) for i in range(size)])  8.42 us
  transfers between devices with their start and end apart: 14, of which 11 were waited for; matrix products, arithmetic and copies ran while one was open for 7% of the time, Pallas kernels for 0%

profile of v1, /device:TPU:16, one launch (start us, length us, event | category | flops | bytes accessed | tf_op | source)
XLA Modules:
  0.0 264.2 jit_solution(16331051741013565432)
XLA Ops:
  7.3 3.4 %collective-permute-start = (s32[30]{0:T(128)S(1)}, s32[30]{0:T(128)S(1)}, u32[]{:S(2)}, u32[]{:S(2)}) collective-permute-start(s32[30]{0:T(128)S(1)} %slice.300), channel_id=1, source_target_pairs={{0,4},{4,8},{8,12},{12,16},{16,20},{20,24},{24,28},{1,5},{5,9},{9,... | collective-permute-start | bytes 368 | tf_op jit(solution)/shard_map/ppermute | solution.py:36
  11.9 3.5 %collective-permute-start.1 = (bf16[30,256]{1,0:T(8,128)(2,1)S(1)}, bf16[30,256]{1,0:T(8,128)(2,1)S(1)}, u32[]{:S(2)}, u32[]{:S(2)}) collective-permute-start(bf16[30,256]{1,0:T(8,128)(2,1)S(1)} %slice.406), channel_id=1, source_target_pairs={{0,4},{4,8},{8,12},{12,16},{16,20},{20,24},{24,28},{1,5},{5,9},{9,... | collective-permute-start | bytes 46088 | tf_op jit(solution)/shard_map/ppermute | solution.py:36
  19.8 4.0 %fusion.17 = f32[512,256]{1,0:T(8,128)S(1)} fusion(f32[542,256]{1,0:T(8,128)S(1)} %maximum_convert_fusion, f32[256]{0:T(256)S(1)} %bitcast.151, f32[256]{0:T(256)S(1)} %bitcast.152, f32[256]{0:T(256)S(1)} %bitcast.123, f32[256]{0:T(256)S(1)} %bitcast.124, f32[256]{0:T(256)S(1)} %bitcast.125, f32[256]{0:T(256)S(1)} %bitcast.126, f32[256]{0:T(256)S(1)} %bitcast.127, ...), kind=kLoop, calls=%fused_computation.23 | loop fusion | flops 11927552 | bytes 16824320 | tf_op jit(solution)/shard_map/add | solution.py:86
  24.8 1.6 multiply_reduce_fusion.1
  27.7 4.0 %fusion.11 = f32[512,2048]{1,0:T(8,128)} fusion(bf16[1024,2048]{1,0:T(8,128)(2,1)} %param.23, s32[]{:T(128)S(6)} %select_n.170, f32[64,8,2,128]{3,2,1,0:T(2,128)S(1)} %bitcast.116, f32[512,256]{1,0:T(8,128)S(1)} %fusion.17, f32[64,8,2,128]{3,2,1,0:T(2,128)S(1)} %bitcast.117, f32[256]{0:T(256)S(1)} %copy-done.5, f32[256]{0:T(256)S(1)} %copy-done.6), kind=kOutput, calls=%fused_computation.16 | convolution fusion | flops 538050560 | bytes 6817796 | tf_op jit(solution)/shard_map/dot_general | solution.py:102
  35.4 41.0 %reduce-scatter.2.cloned.1.call-done = f32[128,2048]{1,0:T(8,128)} async-done(((f32[512,2048]{1,0:T(8,128)}), f32[128,2048]{1,0:T(8,128)}) %reduce-scatter.2.cloned.1.call-update) | async-done | bytes 1048592 | tf_op jit(solution)/shard_map/reduce_scatter | solution.py:101
  78.0 2.1 convolution_convert_fusion
  80.1 6.0 %all-to-all-start = ((bf16[8,64,2048]{2,1,0:T(8,128)(2,1)}), bf16[8,64,2048]{2,1,0:T(8,128)(2,1)S(1)}, u32[]{:S(2)}, u32[]{:S(2)}) async-start(bf16[8,64,2048]{2,1,0:T(8,128)(2,1)} %bitcast.34), calls=%async_computation.1 | async-start | bytes 4194304 | tf_op jit(solution)/shard_map/all_to_all | solution.py:126
  86.4 26.6 %all-gather.7.cloned.1.call-done = bf16[1,2048,1024]{2,1,0:T(8,128)(2,1)} async-done(((bf16[1,2048,256]{2,1,0:T(8,128)(2,1)}), bf16[1,2048,1024]{2,1,0:T(8,128)(2,1)}) %all-gather.7.cloned.1.call-update) | async-done | bytes 4194320 | tf_op jit(solution)/shard_map/all_gather | solution.py:71
  113.0 17.9 %all-to-all-done = bf16[8,64,2048]{2,1,0:T(8,128)(2,1)S(1)} async-done(((bf16[8,64,2048]{2,1,0:T(8,128)(2,1)}), bf16[8,64,2048]{2,1,0:T(8,128)(2,1)S(1)}, u32[]{:S(2)}, u32[]{:S(2)}) %all-to-all-start) | async-done | bytes 2097184 | tf_op jit(solution)/shard_map/all_to_all | solution.py:126
  131.0 6.7 %fusion.4 = f32[512,1024]{1,0:T(8,128)} fusion(bf16[512,2048]{1,0:T(8,128)(2,1)S(1)} %bitcast.120, bf16[1,2048,1024]{2,1,0:T(8,128)(2,1)} %all-gather.7.cloned.1.call-done), kind=kOutput, calls=%fused_computation.7 | convolution fusion | flops 2147483648 | bytes 8388608 | tf_op jit(solution)/shard_map/dot_general | solution.py:129
  137.6 11.5 %all-gather.11.cloned.1.call-done = bf16[1,1024,2048]{2,1,0:T(8,128)(2,1)} async-done(((bf16[1,256,2048]{2,1,0:T(8,128)(2,1)}), bf16[1,1024,2048]{2,1,0:T(8,128)(2,1)}) %all-gather.11.cloned.1.call-update) | async-done | bytes 4194320 | tf_op jit(solution)/shard_map/all_gather | solution.py:74
  149.1 36.4 %all-gather.9.cloned.1.call-done = bf16[1,2048,1024]{2,1,0:T(8,128)(2,1)} async-done(((bf16[1,2048,256]{2,1,0:T(8,128)(2,1)}), bf16[1,2048,1024]{2,1,0:T(8,128)(2,1)}) %all-gather.9.cloned.1.call-update) | async-done | bytes 4194320 | tf_op jit(solution)/shard_map/all_gather | solution.py:72
  185.5 9.2 %fusion.6 = bf16[512,2048]{1,0:T(8,128)(2,1)S(1)} fusion(bf16[1,1024,2048]{2,1,0:T(8,128)(2,1)} %all-gather.11.cloned.1.call-done, f32[512,1024]{1,0:T(8,128)} %fusion.4, bf16[512,2048]{1,0:T(8,128)(2,1)} %bitcast.121, bf16[1,2048,1024]{2,1,0:T(8,128)(2,1)} %all-gather.9.cloned.1.call-done), kind=kOutput, calls=%fused_computation.9 | convolution fusion | flops 4299161600 | bytes 14680064 | tf_op jit(solution)/shard_map/dot_general | solution.py:132
  199.8 3.3 %collective-permute-start.6 = (bf16[1,64,2048]{2,1,0:T(8,128)(2,1)S(1)}, bf16[1,64,2048]{2,1,0:T(8,128)(2,1)S(1)}, u32[]{:S(2)}, u32[]{:S(2)}) collective-permute-start(bf16[1,64,2048]{2,1,0:T(8,128)(2,1)S(1)} %get-tuple-element.10), channel_id=1, source_target_pairs={{0,20},{4,16},{8,28},{12,24},{16,4},{20,0},{24,12},{28,8},{1,21},{... | collective-permute-start | bytes 786440 | tf_op jit(solution)/shard_map/ppermute | solution.py:28
  204.1 10.2 %collective-permute-done.3 = bf16[1,64,2048]{2,1,0:T(8,128)(2,1)S(1)} collective-permute-done((bf16[1,64,2048]{2,1,0:T(8,128)(2,1)S(1)}, bf16[1,64,2048]{2,1,0:T(8,128)(2,1)S(1)}, u32[]{:S(2)}, u32[]{:S(2)}) %collective-permute-start.3) | collective-permute-done | bytes 262176 | tf_op jit(solution)/shard_map/ppermute | solution.py:28
  214.8 4.1 %collective-permute-done.4 = bf16[1,64,2048]{2,1,0:T(8,128)(2,1)S(1)} collective-permute-done((bf16[1,64,2048]{2,1,0:T(8,128)(2,1)S(1)}, bf16[1,64,2048]{2,1,0:T(8,128)(2,1)S(1)}, u32[]{:S(2)}, u32[]{:S(2)}) %collective-permute-start.4) | collective-permute-done | bytes 262176 | tf_op jit(solution)/shard_map/ppermute | solution.py:28
  219.0 15.6 %collective-permute-done.6 = bf16[1,64,2048]{2,1,0:T(8,128)(2,1)S(1)} collective-permute-done((bf16[1,64,2048]{2,1,0:T(8,128)(2,1)S(1)}, bf16[1,64,2048]{2,1,0:T(8,128)(2,1)S(1)}, u32[]{:S(2)}, u32[]{:S(2)}) %collective-permute-start.6) | collective-permute-done | bytes 262176 | tf_op jit(solution)/shard_map/ppermute | solution.py:28
  234.6 8.5 %collective-permute-done.7 = bf16[1,64,2048]{2,1,0:T(8,128)(2,1)S(1)} collective-permute-done((bf16[1,64,2048]{2,1,0:T(8,128)(2,1)S(1)}, bf16[1,64,2048]{2,1,0:T(8,128)(2,1)S(1)}, u32[]{:S(2)}, u32[]{:S(2)}) %collective-permute-start.7) | collective-permute-done | bytes 262176 | tf_op jit(solution)/shard_map/ppermute | solution.py:28
  243.1 5.0 %collective-permute-done.8 = bf16[1,64,2048]{2,1,0:T(8,128)(2,1)S(1)} collective-permute-done((bf16[1,64,2048]{2,1,0:T(8,128)(2,1)S(1)}, bf16[1,64,2048]{2,1,0:T(8,128)(2,1)S(1)}, u32[]{:S(2)}, u32[]{:S(2)}) %collective-permute-start.8) | collective-permute-done | bytes 262176 | tf_op jit(solution)/shard_map/ppermute | solution.py:28
  249.4 2.3 gather_fusion
  251.7 1.7 gather_fusion.1
  253.4 1.7 gather_fusion.2
  255.2 2.5 add_convert_fusion
  (81 shorter events, 21.9 us)
Async XLA Ops:
  6.5 27.2 %copy-start = (s32[512,2]{0,1:T(2,128)S(1)}, s32[512,2]{0,1:T(2,128)}, u32[]{:S(2)}) copy-start(s32[512,2]{0,1:T(2,128)} %param.25) | copy-start | bytes 12292
  6.5 69.9 %reduce-scatter.2.cloned.1.call-start = ((), (), s32[]{:S(2)}) async-start(), calls=%async_computation.2 | async-start | bytes 5242880 | tf_op jit(solution)/shard_map/reduce_scatter | solution.py:101
  7.3 10.1 %collective-permute-start = (s32[30]{0:T(128)S(1)}, s32[30]{0:T(128)S(1)}, u32[]{:S(2)}, u32[]{:S(2)}) collective-permute-start(s32[30]{0:T(128)S(1)} %slice.300), channel_id=1, source_target_pairs={{0,4},{4,8},{8,12},{12,16},{16,20},{20,24},{24,28},{1,5},{5,9},{9,... | collective-permute-start | bytes 368 | tf_op jit(solution)/shard_map/ppermute | solution.py:36
  11.9 7.8 %collective-permute-start.1 = (bf16[30,256]{1,0:T(8,128)(2,1)S(1)}, bf16[30,256]{1,0:T(8,128)(2,1)S(1)}, u32[]{:S(2)}, u32[]{:S(2)}) collective-permute-start(bf16[30,256]{1,0:T(8,128)(2,1)S(1)} %slice.406), channel_id=1, source_target_pairs={{0,4},{4,8},{8,12},{12,16},{16,20},{20,24},{24,28},{1,5},{5,9},{9,... | collective-permute-start | bytes 46088 | tf_op jit(solution)/shard_map/ppermute | solution.py:36
  24.1 3.5 %copy-start.5 = (f32[256]{0:T(256)S(1)}, f32[256]{0:T(256)}, u32[]{:S(2)}) copy-start(f32[256]{0:T(256)} %param.22) | copy-start | bytes 3076
  24.1 3.5 %copy-start.6 = (f32[256]{0:T(256)S(1)}, f32[256]{0:T(256)}, u32[]{:S(2)}) copy-start(f32[256]{0:T(256)} %param.21) | copy-start | bytes 3076
  31.6 81.4 %all-gather.7.cloned.1.call-start = ((), (), s32[]{:S(2)}) async-start(), calls=%async_computation.3 | async-start | bytes 5242880 | tf_op jit(solution)/shard_map/all_gather | solution.py:71
  32.4 45.3 %copy-start.1 = (bf16[128,2048]{1,0:T(8,128)(2,1)S(1)}, bf16[128,2048]{1,0:T(8,128)(2,1)}, u32[]{:S(2)}) copy-start(bf16[128,2048]{1,0:T(8,128)(2,1)} %param.16) | copy-start | bytes 1572868
  32.4 116.7 %all-gather.11.cloned.1.call-start = ((), (), s32[]{:S(2)}) async-start(), calls=%async_computation.5 | async-start | bytes 5242880 | tf_op jit(solution)/shard_map/all_gather | solution.py:74
  33.1 44.9 %copy-start.4 = (f32[2048]{0:T(1024)S(1)}, f32[2048]{0:T(1024)}, u32[]{:S(2)}) copy-start(f32[2048]{0:T(1024)} %param.24) | copy-start | bytes 24580
  33.1 152.4 %all-gather.9.cloned.1.call-start = ((), (), s32[]{:S(2)}) async-start(), calls=%async_computation.4 | async-start | bytes 5242880 | tf_op jit(solution)/shard_map/all_gather | solution.py:72
  80.1 50.8 %all-to-all-start = ((bf16[8,64,2048]{2,1,0:T(8,128)(2,1)}), bf16[8,64,2048]{2,1,0:T(8,128)(2,1)S(1)}, u32[]{:S(2)}, u32[]{:S(2)}) async-start(bf16[8,64,2048]{2,1,0:T(8,128)(2,1)} %bitcast.34), calls=%async_computation.1 | async-start | bytes 4194304 | tf_op jit(solution)/shard_map/all_to_all | solution.py:126
  130.9 6.7 %copy-start.3 = (bf16[8,64,2048]{2,1,0:T(8,128)(2,1)}, bf16[8,64,2048]{2,1,0:T(8,128)(2,1)S(1)}, u32[]{:S(2)}) copy-start(bf16[8,64,2048]{2,1,0:T(8,128)(2,1)S(1)} %all-to-all-done) | copy-start | bytes 6291460
  195.0 8.5 %collective-permute-start.2 = (bf16[1,64,2048]{2,1,0:T(8,128)(2,1)S(1)}, bf16[1,64,2048]{2,1,0:T(8,128)(2,1)S(1)}, u32[]{:S(2)}, u32[]{:S(2)}) collective-permute-start(bf16[1,64,2048]{2,1,0:T(8,128)(2,1)S(1)} %get-tuple-element.14), channel_id=1, source_target_pairs={{0,4},{4,0},{8,12},{12,8},{16,20},{20,16},{24,28},{28,24},{1,5},{5... | collective-permute-start | bytes 786440 | tf_op jit(solution)/shard_map/ppermute | solution.py:28
  197.2 17.1 %collective-permute-start.3 = (bf16[1,64,2048]{2,1,0:T(8,128)(2,1)S(1)}, bf16[1,64,2048]{2,1,0:T(8,128)(2,1)S(1)}, u32[]{:S(2)}, u32[]{:S(2)}) collective-permute-start(bf16[1,64,2048]{2,1,0:T(8,128)(2,1)S(1)} %get-tuple-element.13), channel_id=1, source_target_pairs={{0,8},{4,12},{8,0},{12,4},{16,24},{20,28},{24,16},{28,20},{1,9},{5... | collective-permute-start | bytes 786440 | tf_op jit(solution)/shard_map/ppermute | solution.py:28
  198.7 20.2 %collective-permute-start.4 = (bf16[1,64,2048]{2,1,0:T(8,128)(2,1)S(1)}, bf16[1,64,2048]{2,1,0:T(8,128)(2,1)S(1)}, u32[]{:S(2)}, u32[]{:S(2)}) collective-permute-start(bf16[1,64,2048]{2,1,0:T(8,128)(2,1)S(1)} %get-tuple-element.12), channel_id=1, source_target_pairs={{0,12},{4,8},{8,4},{12,0},{16,28},{20,24},{24,20},{28,16},{1,13},{... | collective-permute-start | bytes 786440 | tf_op jit(solution)/shard_map/ppermute | solution.py:28
  199.2 19.7 %collective-permute-start.5 = (bf16[1,64,2048]{2,1,0:T(8,128)(2,1)S(1)}, bf16[1,64,2048]{2,1,0:T(8,128)(2,1)S(1)}, u32[]{:S(2)}, u32[]{:S(2)}) collective-permute-start(bf16[1,64,2048]{2,1,0:T(8,128)(2,1)S(1)} %get-tuple-element.11), channel_id=1, source_target_pairs={{0,16},{4,20},{8,24},{12,28},{16,0},{20,4},{24,8},{28,12},{1,17},{... | collective-permute-start | bytes 786440 | tf_op jit(solution)/shard_map/ppermute | solution.py:28
  199.8 34.8 %collective-permute-start.6 = (bf16[1,64,2048]{2,1,0:T(8,128)(2,1)S(1)}, bf16[1,64,2048]{2,1,0:T(8,128)(2,1)S(1)}, u32[]{:S(2)}, u32[]{:S(2)}) collective-permute-start(bf16[1,64,2048]{2,1,0:T(8,128)(2,1)S(1)} %get-tuple-element.10), channel_id=1, source_target_pairs={{0,20},{4,16},{8,28},{12,24},{16,4},{20,0},{24,12},{28,8},{1,21},{... | collective-permute-start | bytes 786440 | tf_op jit(solution)/shard_map/ppermute | solution.py:28
  203.5 39.5 %collective-permute-start.7 = (bf16[1,64,2048]{2,1,0:T(8,128)(2,1)S(1)}, bf16[1,64,2048]{2,1,0:T(8,128)(2,1)S(1)}, u32[]{:S(2)}, u32[]{:S(2)}) collective-permute-start(bf16[1,64,2048]{2,1,0:T(8,128)(2,1)S(1)} %get-tuple-element.9), channel_id=1, source_target_pairs={{0,24},{4,28},{8,16},{12,20},{16,8},{20,12},{24,0},{28,4},{1,25},{... | collective-permute-start | bytes 786440 | tf_op jit(solution)/shard_map/ppermute | solution.py:28
  214.3 33.8 %collective-permute-start.8 = (bf16[1,64,2048]{2,1,0:T(8,128)(2,1)S(1)}, bf16[1,64,2048]{2,1,0:T(8,128)(2,1)S(1)}, u32[]{:S(2)}, u32[]{:S(2)}) collective-permute-start(bf16[1,64,2048]{2,1,0:T(8,128)(2,1)S(1)} %get-tuple-element.8), channel_id=1, source_target_pairs={{0,28},{4,24},{8,20},{12,16},{16,12},{20,8},{24,4},{28,0},{1,29},{... | collective-permute-start | bytes 786440 | tf_op jit(solution)/shard_map/ppermute | solution.py:28
  248.1 1.4 copy-start.2
Sparse Core Ops, SparseCore 0:
  31.8 44.6 reduce-scatter.1
  78.0 35.0 all-gather.6
  114.6 34.4 all-gather.10
  150.5 34.9 all-gather.8
